TPU v7x, 32 devices: a whole 2x2x4 slice. The times are simulated.
32 devices in a mesh: ep: 8 (over z, x), tp: 4 (over y, core).
Axes of the slice: x: 2, y: 2, z: 4, core: 2. Of those that a mesh axis runs over, the one named last changes fastest.
Arguments:
- residual: bfloat16 [256, 2048], P('ep'), may hold values from -6 to 6
- routes: int32 [256, 4], P('ep'), may hold values from 0 to 7, as said below
- lengths: int32 [256], P('ep'), may hold values from 1 to 512, as said below
- key_cache: bfloat16 [256, 512, 4, 128], P('ep', None, 'tp'), may hold values from -6 to 6
- value_cache: bfloat16 [256, 512, 4, 128], P('ep', None, 'tp'), may hold values from -6 to 6
- mix_gain: float32 [2048], replicated, may hold values from 0.1 to 1.9
- w_query: bfloat16 [2048, 2048], P(None, 'tp'), may hold values from -0.125 to 0.125
- w_out: bfloat16 [2048, 2048], P('tp'), may hold values from -0.375 to 0.375
- head_bias: float32 [16], P('tp'), may hold values from -7 to -1
- moe_gain: float32 [2048], replicated, may hold values from 0.1 to 1.9
- w_group: bfloat16 [2048, 1], replicated, may hold values from -0.02734375 to 0.02734375
- w_expert: bfloat16 [2048, 8], replicated, may hold values from -0.02734375 to 0.02734375
- expert_gate: bfloat16 [8, 2048, 1024], P('ep', None, 'tp'), may hold values from -0.125 to 0.125
- expert_up: bfloat16 [8, 2048, 1024], P('ep', None, 'tp'), may hold values from -0.125 to 0.125
- expert_down: bfloat16 [8, 1024, 2048], P('ep', 'tp'), may hold values from -3 to 3
Outputs:
- layer_out: bfloat16 [256, 2048], P('ep', 'tp')
Inputs may be any that keep to these rules, and one draw needn't show every extreme that they name: `routes`: each row names 4 different experts, all in one group of 8 consecutive experts. Within the rows of one device (aligned blocks of 32 rows) no expert is named more than 16 times, and some expert is named exactly 16 times in every block. `lengths`: some sequence has 512 cached positions in every draw.
All inputs are finite; a program needn't handle non-finite values.
Results may differ from a plain program's by a relative error of at most 0.02.
Values may be sent and summed in bfloat16 or wider, within the bound.
A program may use at most 64 MiB of HBM per device.

v0:
```python
import jax
import jax.numpy as jnp
from jax import lax
from jax.sharding import PartitionSpec as P

GROUP_SIZE = 8
TOPK = 4
EPSILON = 1e-06


def rms_scale(tokens, gains):
    values = tokens.astype(jnp.float32)
    inverse = lax.rsqrt(jnp.mean(values * values, axis=-1, keepdims=True) + EPSILON)
    return (values * inverse * gains).astype(jnp.bfloat16)


def stick_read(queries, key_rows, value_rows, head_bias, lengths):
    seq_count = queries.shape[0]
    key_heads = key_rows.shape[2]
    head_size = key_rows.shape[3]
    per_key = head_bias.shape[0] // key_heads
    grouped = queries.reshape(seq_count, key_heads, per_key, head_size)
    scores = jnp.einsum(
        "tkgd,tlkd->tkgl", grouped, key_rows, preferred_element_type=jnp.float32
    ) * head_size ** (-0.5)
    scores = scores + head_bias.reshape(1, key_heads, per_key, 1)
    inside = lax.broadcasted_iota(jnp.int32, scores.shape, 3) < lengths[:, None, None, None]
    remain = jnp.where(inside, jax.nn.log_sigmoid(-scores), 0.0)
    later_sum = lax.cumsum(remain, axis=3, reverse=True) - remain
    weights = jnp.where(inside, jnp.exp(jax.nn.log_sigmoid(scores) + later_sum), 0.0).astype(
        jnp.bfloat16
    )
    mixture = jnp.einsum("tkgl,tlkd->tkgd", weights, value_rows, preferred_element_type=jnp.float32)
    return mixture.astype(jnp.bfloat16).reshape(seq_count, key_heads * per_key * head_size)


def per_device(
    residual,
    routes,
    lengths,
    key_cache,
    value_cache,
    mix_gain,
    w_query,
    w_out,
    head_bias,
    moe_gain,
    w_group,
    w_expert,
    expert_gate,
    expert_up,
    expert_down,
):
    seq_count = residual.shape[0]
    width = residual.shape[1]
    own_width = width // lax.axis_size("tp")
    own_start = lax.axis_index("tp") * own_width
    normed = rms_scale(residual, mix_gain)
    queries = jnp.dot(normed, w_query, preferred_element_type=jnp.float32).astype(jnp.bfloat16)
    attended = stick_read(queries, key_cache, value_cache, head_bias, lengths)
    head_part = (
        jnp.dot(attended, w_out, preferred_element_type=jnp.float32)
        .astype(jnp.bfloat16)
        .astype(jnp.float32)
    )
    attn_own = lax.psum_scatter(
        head_part.astype(jnp.bfloat16), "tp", scatter_dimension=1, tiled=True
    )
    res_own = lax.dynamic_slice_in_dim(residual, own_start, own_width, 1)
    mid_own = (res_own.astype(jnp.float32) + attn_own.astype(jnp.float32)).astype(jnp.bfloat16)
    mid_values = mid_own.astype(jnp.float32)
    squares = lax.psum(jnp.sum(mid_values * mid_values, axis=1), "tp")
    inverse = lax.rsqrt(squares / width + EPSILON)
    gain_own = lax.dynamic_slice_in_dim(moe_gain, own_start, own_width, 0)
    send_rows = (mid_values * inverse[:, None] * gain_own[None, :]).astype(jnp.bfloat16)
    hidden_in = lax.all_gather(send_rows, "tp", axis=1, tiled=True)
    expert_count = w_expert.shape[1]
    group_count = w_group.shape[1]
    group_prob = jax.nn.softmax(
        jnp.dot(hidden_in, w_group, preferred_element_type=jnp.float32), axis=-1
    )
    expert_logit = jnp.dot(hidden_in, w_expert, preferred_element_type=jnp.float32)
    expert_ids = jnp.arange(expert_count, dtype=jnp.int32)
    chosen = routes[:, :, None] == expert_ids[None, None, :]
    picked = jnp.sum(jnp.where(chosen, expert_logit[:, None, :], 0.0), axis=2)
    group_hot = routes[:, :1] // GROUP_SIZE == jnp.arange(group_count, dtype=jnp.int32)[None, :]
    top_prob = jnp.sum(jnp.where(group_hot, group_prob, 0.0), axis=1, keepdims=True)
    share = jax.nn.softmax(picked, axis=1) * top_prob
    group_most = min(seq_count, max(4, 2 * seq_count // group_count))
    capacity = group_most * TOPK // GROUP_SIZE
    flat_hot = chosen.reshape(seq_count * TOPK, expert_count).astype(jnp.int32)
    earlier = jnp.cumsum(flat_hot, axis=0, dtype=jnp.int32) - flat_hot
    slot = jnp.sum(earlier * flat_hot, axis=1, dtype=jnp.int32)
    target = routes.reshape(-1) * capacity + slot
    placing = target[:, None] == jnp.arange(expert_count * capacity, dtype=jnp.int32)[None, :]
    placing = placing.reshape(seq_count, TOPK, expert_count * capacity)
    token_place = jnp.sum(placing.astype(jnp.int32), axis=1).astype(jnp.bfloat16)
    outgoing = jnp.einsum("sq,sd->qd", token_place, send_rows, preferred_element_type=jnp.float32)
    outgoing = outgoing.astype(jnp.bfloat16).reshape(expert_count, capacity, send_rows.shape[1])
    local_experts = expert_gate.shape[0]
    arrived = lax.all_to_all(outgoing, "ep", split_axis=0, concat_axis=0, tiled=True)
    arrived = lax.all_gather(arrived, "tp", axis=2, tiled=True)
    sources = arrived.shape[0] // local_experts
    batch_rows = arrived.reshape(sources, local_experts, arrived.shape[1], arrived.shape[2])
    gate = jnp.einsum("nxcd,xdf->nxcf", batch_rows, expert_gate, preferred_element_type=jnp.float32)
    upward = jnp.einsum("nxcd,xdf->nxcf", batch_rows, expert_up, preferred_element_type=jnp.float32)
    active = (jax.nn.silu(gate) * upward).astype(jnp.bfloat16)
    partial_value = jnp.einsum(
        "nxcf,xfd->nxcd", active, expert_down, preferred_element_type=jnp.float32
    )
    partial_value = partial_value.astype(jnp.bfloat16).astype(jnp.float32)
    partial_value = partial_value.reshape(
        arrived.shape[0], arrived.shape[1], partial_value.shape[3]
    )
    summed = lax.psum_scatter(
        partial_value.astype(jnp.bfloat16), "tp", scatter_dimension=2, tiled=True
    )
    returned = lax.all_to_all(summed, "ep", split_axis=0, concat_axis=0, tiled=True)
    combine = jnp.einsum(
        "sk,skq->sq", share, placing.astype(jnp.float32), precision=lax.Precision.HIGHEST
    )
    moe = jnp.dot(
        combine,
        returned.reshape(expert_count * capacity, own_width).astype(jnp.float32),
        precision=lax.Precision.HIGHEST,
    )
    return (mid_own.astype(jnp.float32) + moe).astype(jnp.bfloat16)


def solution(mesh):
    in_specs = (
        P("ep", None),
        P("ep", None),
        P("ep"),
        P("ep", None, "tp", None),
        P("ep", None, "tp", None),
        P(),
        P(None, "tp"),
        P("tp", None),
        P("tp"),
        P(),
        P(),
        P(),
        P("ep", None, "tp"),
        P("ep", None, "tp"),
        P("ep", "tp", None),
    )
    out_specs = P("ep", "tp")
    return jax.shard_map(
        per_device, mesh=mesh, in_specs=in_specs, out_specs=out_specs, check_vma=False
    )
```

profile of v0, /device:TPU:0, one launch (start us, length us, event | category | flops | bytes accessed | tf_op | source)
XLA Modules:
  0.0 132.4 jit_solution(12256758625774551817)
XLA Ops:
  6.5 1.2 fusion.28
  7.7 2.2 %convolution_convert_fusion.3 = bf16[32,512]{1,0:T(8,128)(2,1)S(1)} fusion(bf16[2048,512]{1,0:T(8,128)(2,1)} %param.21, bf16[32,2048]{1,0:T(8,128)(2,1)} %param.15, f32[2048]{0:T(1024)} %param.20, f32[32]{0:T(128)S(1)} %add_rsqrt_fusion.1), kind=kOutput, calls=%fused_computation.16 | convolution fusion | flops 67387392 | bytes 2269312 | tf_op jit(solution)/shard_map/dot_general | solution.py:59
  10.0 3.4 %fusion.37 = (f32[32,4,512]{2,1,0:T(4,128)S(1)}, f32[32,4,512]{2,1,0:T(4,128)S(1)}) fusion(s32[32]{0:T(128)} %param.17, f32[4]{0:T(128)} %param.23, bf16[32,4,128]{2,1,0:T(4,128)(2,1)S(1)} %reshape.157, bf16[32,512,1,128]{3,1,2,0:T(8,128)(2,1)} %param.18), kind=kOutput, calls=%fused_computation.41 | convolution fusion | flops 17498112 | bytes 4751504 | tf_op jit(solution)/shard_map/tkgd,tlkd->tkgl/dot_general | solution.py:23
  13.4 0.2 reshape.159
  13.7 19.9 %reduce-window.6 = f32[32,1,4,4,128]{4,0,2,1,3:T(8,128)S(1)} reduce-window(f32[32,1,4,4,128]{4,0,2,1,3:T(8,128)S(1)} %copy.41, f32[]{:T(128)} %constant.45.clone.1), window={size=1x1x1x1x128 pad=0_0x0_0x0_0x0_0x0_127}, to_apply=%region_1.2 | reduce-window | flops 8323072 | bytes 524292 | tf_op jit(solution)/shard_map/reduce-window
  33.6 0.2 copy.42
  33.8 0.2 copy.43
  34.0 0.1 copy.44
  34.1 0.2 broadcast.61
  34.3 0.2 reshape.163
  34.5 0.2 reshape.160
  34.7 3.2 %fusion.14 = bf16[32,4,128]{2,1,0:T(4,128)(2,1)S(1)} fusion(bf16[32,512,1,128]{3,1,2,0:T(8,128)(2,1)} %param.19, f32[32,4,512]{2,1,0:T(4,128)S(1)} %reshape.160, f32[32,4,512]{2,1,0:T(4,128)S(1)} %reshape.163, f32[32,4,512]{2,1,0:T(4,128)S(1)} %get-tuple-element.8, s32[32]{0:T(128)S(1)} %copy-done.3), kind=kOutput, calls=%fused_computation.17 | convolution fusion | flops 18235392 | bytes 5013632 | tf_op jit(solution)/shard_map/tkgl,tlkd->tkgd/dot_general | solution.py:33
  37.9 1.1 convolution_convert_fusion.1
  39.4 0.2 reduce_window_sum.25
  39.6 0.2 select_reduce_fusion
  39.9 0.8 dynamic_slice.7
  40.8 20.8 %reduce-scatter.3.cloned.1.call-done = bf16[32,512]{1,0:T(8,128)(2,1)} async-done(((bf16[32,2048]{1,0:T(8,128)(2,1)}), bf16[32,512]{1,0:T(8,128)(2,1)}) %reduce-scatter.3.cloned.1.call-update) | async-done | bytes 32784 | tf_op jit(solution)/shard_map/reduce_scatter | solution.py:66
  61.6 0.9 fusion.49
  62.5 5.8 %psum.7 = f32[32]{0:T(128)S(1)} all-reduce(f32[32]{0:T(128)S(1)} %get-tuple-element.5), channel_id=1, replica_groups=mesh['ep'=8,'tp'=4] {'tp'}, use_global_device_ids=true, to_apply=%region_5.6 | all-reduce | flops 32 | bytes 256 | tf_op jit(solution)/shard_map/psum | solution.py:72
  68.3 0.2 convolution_convert_fusion.2
  68.6 12.8 %all_to_all.10 = bf16[8,16,512]{2,1,0:T(8,128)(2,1)S(1)} all-to-all(bf16[8,16,512]{2,1,0:T(8,128)(2,1)S(1)} %bitcast.105), channel_id=1, replica_groups=mesh['ep'=8,'tp'=4] {'ep'}, dimensions={0} | all-to-all | bytes 262144 | tf_op jit(solution)/shard_map/all_to_all | solution.py:101
  81.4 6.5 %all_gather.7 = bf16[8,16,2048]{2,1,0:T(8,128)(2,1)S(1)} all-gather(bf16[8,16,512]{2,1,0:T(8,128)(2,1)S(1)} %all_to_all.10), channel_id=1, replica_groups=mesh['ep'=8,'tp'=4] {'tp'}, dimensions={2}, use_global_device_ids=true | all-gather | bytes 655360 | tf_op jit(solution)/shard_map/all_gather | solution.py:102
  87.9 1.5 %convolution_bitcast_fusion.1 = f32[8,1,16,256]{3,2,0,1:T(8,128)S(1)} fusion(bf16[8,16,2048]{2,1,0:T(8,128)(2,1)S(1)} %all_gather.7, bf16[1,2048,256]{2,1,0:T(8,128)(2,1)} %param.27), kind=kOutput, calls=%fused_computation.11 | convolution fusion | flops 134217728 | bytes 1703936 | tf_op jit(solution)/shard_map/nxcd,xdf->nxcf/dot_general | solution.py:105
  89.4 3.1 %convolution_convert_fusion = bf16[8,16,2048]{2,1,0:T(8,128)(2,1)} fusion(bf16[1,256,2048]{2,1,0:T(8,128)(2,1)} %param.29, bf16[8,16,2048]{2,1,0:T(8,128)(2,1)S(1)} %all_gather.7, bf16[1,2048,256]{2,1,0:T(8,128)(2,1)} %param.28, f32[8,1,16,256]{3,2,0,1:T(8,128)S(1)} %convolution_bitcast_fusion.1), kind=kOutput, calls=%fused_computation.4 | convolution fusion | flops 268894208 | bytes 3276800 | tf_op jit(solution)/shard_map/nxcf,xfd->nxcd/dot_general | solution.py:108
  92.6 5.4 %all_gather.6 = bf16[32,2048]{1,0:T(8,128)(2,1)S(1)} all-gather(bf16[32,512]{1,0:T(8,128)(2,1)S(1)} %fusion.51), channel_id=1, replica_groups=mesh['ep'=8,'tp'=4] {'tp'}, dimensions={1}, use_global_device_ids=true | all-gather | bytes 163840 | tf_op jit(solution)/shard_map/all_gather | solution.py:76
  98.1 0.1 fusion.63
  98.3 0.2 fusion.22
  98.4 13.4 %reduce-scatter.5.cloned.1.call-done = bf16[8,16,512]{2,1,0:T(8,128)(2,1)} async-done(((bf16[8,16,2048]{2,1,0:T(8,128)(2,1)}), bf16[8,16,512]{2,1,0:T(8,128)(2,1)}) %reduce-scatter.5.cloned.1.call-update) | async-done | bytes 131088 | tf_op jit(solution)/shard_map/reduce_scatter | solution.py:115
  111.9 5.5 %all-to-all-start.1 = ((bf16[8,16,512]{2,1,0:T(8,128)(2,1)}), bf16[8,16,512]{2,1,0:T(8,128)(2,1)S(1)}, u32[]{:S(2)}, u32[]{:S(2)}) async-start(bf16[8,16,512]{2,1,0:T(8,128)(2,1)} %reduce-scatter.5.cloned.1.call-done), calls=%async_computation.3 | async-start | bytes 262144 | tf_op jit(solution)/shard_map/all_to_all | solution.py:118
  117.5 0.2 fusion.54
  117.7 7.0 %all-to-all-done.1 = bf16[8,16,512]{2,1,0:T(8,128)(2,1)S(1)} async-done(((bf16[8,16,512]{2,1,0:T(8,128)(2,1)}), bf16[8,16,512]{2,1,0:T(8,128)(2,1)S(1)}, u32[]{:S(2)}, u32[]{:S(2)}) %all-to-all-start.1) | async-done | bytes 131104 | tf_op jit(solution)/shard_map/all_to_all | solution.py:118
  124.7 0.8 fusion.13
  (34 shorter events, 1.2 us)
Async XLA Ops:
  6.5 31.3 %copy-start = (bf16[512,2048]{1,0:T(8,128)(2,1)S(1)}, bf16[512,2048]{1,0:T(8,128)(2,1)}, u32[]{:S(2)}) copy-start(bf16[512,2048]{1,0:T(8,128)(2,1)} %param.22) | copy-start | bytes 6291460
  6.5 55.1 %reduce-scatter.3.cloned.1.call-start = ((), (), s32[]{:S(2)}) async-start(), calls=%async_computation.4 | async-start | bytes 163840 | tf_op jit(solution)/shard_map/reduce_scatter | solution.py:66
  10.0 24.7 %copy-start.3 = (s32[32]{0:T(128)S(1)}, s32[32]{0:T(128)}, u32[]{:S(2)}) copy-start(s32[32]{0:T(128)} %param.17) | copy-start | bytes 388
  34.6 4.5 %copy-start.2 = (s32[32,4]{0,1:T(4,128)S(1)}, s32[32,4]{0,1:T(4,128)}, u32[]{:S(2)}) copy-start(s32[32,4]{0,1:T(4,128)} %param.16) | copy-start | bytes 1540
  39.0 59.1 %copy-start.1 = (bf16[2048,8]{0,1:T(8,128)(2,1)S(1)}, bf16[2048,8]{0,1:T(8,128)(2,1)}, u32[]{:S(2)}) copy-start(bf16[2048,8]{0,1:T(8,128)(2,1)} %param.26) | copy-start | bytes 98308
  39.0 59.3 %copy-start.4 = (bf16[2048,1]{0,1:T(2,128)(2,1)S(1)}, bf16[2048,1]{0,1:T(2,128)(2,1)}, u32[]{:S(2)}) copy-start(bf16[2048,1]{0,1:T(2,128)(2,1)} %param.25) | copy-start | bytes 12292
  39.0 72.8 %reduce-scatter.5.cloned.1.call-start = ((), (), s32[]{:S(2)}) async-start(), calls=%async_computation.5 | async-start | bytes 655360 | tf_op jit(solution)/shard_map/reduce_scatter | solution.py:115
  111.9 12.8 %all-to-all-start.1 = ((bf16[8,16,512]{2,1,0:T(8,128)(2,1)}), bf16[8,16,512]{2,1,0:T(8,128)(2,1)S(1)}, u32[]{:S(2)}, u32[]{:S(2)}) async-start(bf16[8,16,512]{2,1,0:T(8,128)(2,1)} %reduce-scatter.5.cloned.1.call-done), calls=%async_computation.3 | async-start | bytes 262144 | tf_op jit(solution)/shard_map/all_to_all | solution.py:118
Sparse Core Ops, SparseCore 0:
  39.1 22.4 reduce-scatter.2
  92.7 19.1 reduce-scatter.4
where the time goes:
time: 133 us; the launch traced here: 132 us
  waiting for transfers between devices  41.3 us (31%)
  blocking collectives  30.5 us (23%)
  other arithmetic  22.8 us (17%)
  matrix products  16.2 us (12%)
  between operations  13.6 us (10%)
  starting transfers between devices  5.54 us (4%)
  local copies, waits for them, and re-layouts  2.47 us (2%)
    reduce_scatter x1, waiting for transfers between devices, per_device(): lax.psum_scatter(head_part.astype(jnp.bfloat16), 'tp', scatter_dimension=...  20.8 us
    another operation x2, other arithmetic  20 us
    reduce_scatter x1, waiting for transfers between devices, per_device(): lax.psum_scatter(partial_value.astype(jnp.bfloat16), 'tp', scatter_dimens...  13.4 us
    all_to_all x1, blocking collectives, per_device(): lax.all_to_all(outgoing, 'ep', split_axis=0, concat_axis=0, tiled=True)  12.8 us
    all_to_all x1, waiting for transfers between devices, per_device(): lax.all_to_all(summed, 'ep', split_axis=0, concat_axis=0, tiled=True)  6.99 us
    all_gather x1, blocking collectives, per_device(): arrived = lax.all_gather(arrived, 'tp', axis=2, tiled=True)  6.49 us
    psum x1, blocking collectives, per_device(): squares = lax.psum(jnp.sum(mid_values * mid_values, axis=1), 'tp')  5.76 us
    all_to_all x1, starting transfers between devices, per_device(): lax.all_to_all(summed, 'ep', split_axis=0, concat_axis=0, tiled=True)  5.5 us
  transfers between devices with their start and end apart: 3, of which 3 were waited for; matrix products, arithmetic and copies ran while one was open for 2% of the time, Pallas kernels for 0%

commit v1 on v0

--- a/solution.py
+++ b/solution.py
@@ -69,7 +69,7 @@
     res_own = lax.dynamic_slice_in_dim(residual, own_start, own_width, 1)
     mid_own = (res_own.astype(jnp.float32) + attn_own.astype(jnp.float32)).astype(jnp.bfloat16)
     mid_values = mid_own.astype(jnp.float32)
-    squares = lax.psum(jnp.sum(mid_values * mid_values, axis=1), "tp")
+    squares = jnp.sum(lax.all_gather(jnp.sum(mid_values * mid_values, axis=1), "tp"), axis=0)
     inverse = lax.rsqrt(squares / width + EPSILON)
     gain_own = lax.dynamic_slice_in_dim(moe_gain, own_start, own_width, 0)
     send_rows = (mid_values * inverse[:, None] * gain_own[None, :]).astype(jnp.bfloat16)

time: 133 us -> 133 us (level)
    psum x1 -> x0, blocking collectives: 5.76 us -> none  [per_device(): squares = lax.psum(jnp.sum(mid_values * mid_values, axis=1), 'tp')]
    unnamed x0 -> x1, blocking collectives: none -> 5.73 us
where the time goes in v1:
time: 133 us
  waiting for transfers between devices  40 us (30%)
  blocking collectives  30.4 us (23%)
  other arithmetic  22.9 us (17%)
  matrix products  16.2 us (12%)
  between operations  14.3 us (11%)
  starting transfers between devices  5.54 us (4%)
  local copies, waits for them, and re-layouts  3.39 us (3%)
    another operation x2, other arithmetic  20 us
    reduce_scatter x1, waiting for transfers between devices, per_device(): lax.psum_scatter(head_part.astype(jnp.bfloat16), 'tp', scatter_dimension=...  19.6 us
    reduce_scatter x1, waiting for transfers between devices, per_device(): lax.psum_scatter(partial_value.astype(jnp.bfloat16), 'tp', scatter_dimens...  13.4 us
    all_to_all x1, blocking collectives, per_device(): lax.all_to_all(outgoing, 'ep', split_axis=0, concat_axis=0, tiled=True)  12.8 us
    all_to_all x1, waiting for transfers between devices, per_device(): lax.all_to_all(summed, 'ep', split_axis=0, concat_axis=0, tiled=True)  6.99 us
    all_gather x1, blocking collectives, per_device(): arrived = lax.all_gather(arrived, 'tp', axis=2, tiled=True)  6.49 us
    unnamed x1, blocking collectives  5.73 us
    all_to_all x1, starting transfers between devices, per_device(): lax.all_to_all(summed, 'ep', split_axis=0, concat_axis=0, tiled=True)  5.5 us
  transfers between devices with their start and end apart: 3, of which 3 were waited for; matrix products, arithmetic and copies ran while one was open for 2% of the time, Pallas kernels for 0%

profile of v1, /device:TPU:0, one launch (start us, length us, event | category | flops | bytes accessed | tf_op | source)
XLA Modules:
  0.0 132.7 jit_solution(10757813296367577478)
XLA Ops:
  6.5 1.2 fusion.28
  7.7 2.2 %convolution_convert_fusion.3 = bf16[32,512]{1,0:T(8,128)(2,1)S(1)} fusion(bf16[2048,512]{1,0:T(8,128)(2,1)} %param.21, bf16[32,2048]{1,0:T(8,128)(2,1)} %param.15, f32[2048]{0:T(1024)} %param.20, f32[32]{0:T(128)S(1)} %add_rsqrt_fusion.1), kind=kOutput, calls=%fused_computation.16 | convolution fusion | flops 67387392 | bytes 2269312 | tf_op jit(solution)/shard_map/dot_general | solution.py:59
  10.0 3.4 %fusion.37 = (f32[32,4,512]{2,1,0:T(4,128)S(1)}, f32[32,4,512]{2,1,0:T(4,128)S(1)}) fusion(s32[32]{0:T(128)} %param.17, f32[4]{0:T(128)} %param.23, bf16[32,4,128]{2,1,0:T(4,128)(2,1)S(1)} %reshape.161, bf16[32,512,1,128]{3,1,2,0:T(8,128)(2,1)} %param.18), kind=kOutput, calls=%fused_computation.41 | convolution fusion | flops 17498112 | bytes 4751504 | tf_op jit(solution)/shard_map/tkgd,tlkd->tkgl/dot_general | solution.py:23
  13.4 0.2 reshape.163
  13.7 19.9 %reduce-window.6 = f32[32,1,4,4,128]{4,0,2,1,3:T(8,128)S(1)} reduce-window(f32[32,1,4,4,128]{4,0,2,1,3:T(8,128)S(1)} %copy.41, f32[]{:T(128)} %constant.45.clone.1), window={size=1x1x1x1x128 pad=0_0x0_0x0_0x0_0x0_127}, to_apply=%region_1.2 | reduce-window | flops 8323072 | bytes 524292 | tf_op jit(solution)/shard_map/reduce-window
  33.6 0.2 copy.42
  33.8 0.2 copy.43
  34.1 0.2 broadcast.68
  34.3 0.2 reshape.167
  34.5 0.2 reshape.164
  34.7 3.2 %fusion.14 = bf16[32,4,128]{2,1,0:T(4,128)(2,1)S(1)} fusion(bf16[32,512,1,128]{3,1,2,0:T(8,128)(2,1)} %param.19, f32[32,4,512]{2,1,0:T(4,128)S(1)} %reshape.164, f32[32,4,512]{2,1,0:T(4,128)S(1)} %reshape.167, f32[32,4,512]{2,1,0:T(4,128)S(1)} %get-tuple-element.8, s32[32]{0:T(128)S(1)} %copy-done.3), kind=kOutput, calls=%fused_computation.17 | convolution fusion | flops 18235392 | bytes 5013632 | tf_op jit(solution)/shard_map/tkgl,tlkd->tkgd/dot_general | solution.py:33
  37.9 1.1 convolution_convert_fusion.1
  39.4 0.2 reduce_window_sum.25
  39.6 0.2 select_reduce_fusion
  39.9 0.6 dynamic-slice
  41.2 0.8 dynamic_slice.7
  42.1 19.6 %reduce-scatter.3.cloned.1.call-done = bf16[32,512]{1,0:T(8,128)(2,1)} async-done(((bf16[32,2048]{1,0:T(8,128)(2,1)}), bf16[32,512]{1,0:T(8,128)(2,1)}) %reduce-scatter.3.cloned.1.call-update) | async-done | bytes 32784 | tf_op jit(solution)/shard_map/reduce_scatter | solution.py:66
  61.6 0.9 fusion.49
  62.5 0.2 dynamic-update-slice
  62.8 5.7 %all-reduce = f32[128]{0:T(128)S(1)} all-reduce(f32[128]{0:T(128)S(1)} %dynamic-update-slice), channel_id=2, replica_groups=mesh['ep'=8,'tp'=4] {'tp'}, use_global_device_ids=true, to_apply=%add | all-reduce | flops 128 | bytes 1024
  68.7 0.2 convolution_convert_fusion.2
  68.9 12.8 %all_to_all.10 = bf16[8,16,512]{2,1,0:T(8,128)(2,1)S(1)} all-to-all(bf16[8,16,512]{2,1,0:T(8,128)(2,1)S(1)} %bitcast.106), channel_id=1, replica_groups=mesh['ep'=8,'tp'=4] {'ep'}, dimensions={0} | all-to-all | bytes 262144 | tf_op jit(solution)/shard_map/all_to_all | solution.py:101
  81.7 6.5 %all_gather.15 = bf16[8,16,2048]{2,1,0:T(8,128)(2,1)S(1)} all-gather(bf16[8,16,512]{2,1,0:T(8,128)(2,1)S(1)} %all_to_all.10), channel_id=1, replica_groups=mesh['ep'=8,'tp'=4] {'tp'}, dimensions={2}, use_global_device_ids=true | all-gather | bytes 655360 | tf_op jit(solution)/shard_map/all_gather | solution.py:102
  88.2 1.5 %convolution_bitcast_fusion.1 = f32[8,1,16,256]{3,2,0,1:T(8,128)S(1)} fusion(bf16[8,16,2048]{2,1,0:T(8,128)(2,1)S(1)} %all_gather.15, bf16[1,2048,256]{2,1,0:T(8,128)(2,1)} %param.27), kind=kOutput, calls=%fused_computation.11 | convolution fusion | flops 134217728 | bytes 1703936 | tf_op jit(solution)/shard_map/nxcd,xdf->nxcf/dot_general | solution.py:105
  89.7 3.1 %convolution_convert_fusion = bf16[8,16,2048]{2,1,0:T(8,128)(2,1)} fusion(bf16[1,256,2048]{2,1,0:T(8,128)(2,1)} %param.29, bf16[8,16,2048]{2,1,0:T(8,128)(2,1)S(1)} %all_gather.15, bf16[1,2048,256]{2,1,0:T(8,128)(2,1)} %param.28, f32[8,1,16,256]{3,2,0,1:T(8,128)S(1)} %convolution_bitcast_fusion.1), kind=kOutput, calls=%fused_computation.4 | convolution fusion | flops 268894208 | bytes 3276800 | tf_op jit(solution)/shard_map/nxcf,xfd->nxcd/dot_general | solution.py:108
  93.0 5.4 %all_gather.14 = bf16[32,2048]{1,0:T(8,128)(2,1)S(1)} all-gather(bf16[32,512]{1,0:T(8,128)(2,1)S(1)} %fusion.51), channel_id=1, replica_groups=mesh['ep'=8,'tp'=4] {'tp'}, dimensions={1}, use_global_device_ids=true | all-gather | bytes 163840 | tf_op jit(solution)/shard_map/all_gather | solution.py:76
  98.6 0.2 fusion.22
  98.8 13.4 %reduce-scatter.5.cloned.1.call-done = bf16[8,16,512]{2,1,0:T(8,128)(2,1)} async-done(((bf16[8,16,2048]{2,1,0:T(8,128)(2,1)}), bf16[8,16,512]{2,1,0:T(8,128)(2,1)}) %reduce-scatter.5.cloned.1.call-update) | async-done | bytes 131088 | tf_op jit(solution)/shard_map/reduce_scatter | solution.py:115
  112.2 5.5 %all-to-all-start.1 = ((bf16[8,16,512]{2,1,0:T(8,128)(2,1)}), bf16[8,16,512]{2,1,0:T(8,128)(2,1)S(1)}, u32[]{:S(2)}, u32[]{:S(2)}) async-start(bf16[8,16,512]{2,1,0:T(8,128)(2,1)} %reduce-scatter.5.cloned.1.call-done), calls=%async_computation.3 | async-start | bytes 262144 | tf_op jit(solution)/shard_map/all_to_all | solution.py:118
  117.8 0.2 fusion.54
  118.1 7.0 %all-to-all-done.1 = bf16[8,16,512]{2,1,0:T(8,128)(2,1)S(1)} async-done(((bf16[8,16,512]{2,1,0:T(8,128)(2,1)}), bf16[8,16,512]{2,1,0:T(8,128)(2,1)S(1)}, u32[]{:S(2)}, u32[]{:S(2)}) %all-to-all-start.1) | async-done | bytes 131104 | tf_op jit(solution)/shard_map/all_to_all | solution.py:118
  125.0 0.8 fusion.13
  (41 shorter events, 1.5 us)
Async XLA Ops:
  6.5 31.4 %copy-start = (bf16[512,2048]{1,0:T(8,128)(2,1)S(1)}, bf16[512,2048]{1,0:T(8,128)(2,1)}, u32[]{:S(2)}) copy-start(bf16[512,2048]{1,0:T(8,128)(2,1)} %param.22) | copy-start | bytes 6291460
  6.5 55.1 %reduce-scatter.3.cloned.1.call-start = ((), (), s32[]{:S(2)}) async-start(), calls=%async_computation.4 | async-start | bytes 163840 | tf_op jit(solution)/shard_map/reduce_scatter | solution.py:66
  10.0 24.7 %copy-start.3 = (s32[32]{0:T(128)S(1)}, s32[32]{0:T(128)}, u32[]{:S(2)}) copy-start(s32[32]{0:T(128)} %param.17) | copy-start | bytes 388
  34.6 4.5 %copy-start.2 = (s32[32,4]{0,1:T(4,128)S(1)}, s32[32,4]{0,1:T(4,128)}, u32[]{:S(2)}) copy-start(s32[32,4]{0,1:T(4,128)} %param.16) | copy-start | bytes 1540
  34.7 5.3 %copy-start.5 = (u32[32]{0:T(128)S(1)}, u32[32]{0:T(128)}, u32[]{:S(2)}) copy-start(u32[32]{0:T(128)} %constant.63) | copy-start | bytes 388
  39.0 59.4 %copy-start.1 = (bf16[2048,8]{0,1:T(8,128)(2,1)S(1)}, bf16[2048,8]{0,1:T(8,128)(2,1)}, u32[]{:S(2)}) copy-start(bf16[2048,8]{0,1:T(8,128)(2,1)} %param.26) | copy-start | bytes 98308
  39.0 59.6 %copy-start.4 = (bf16[2048,1]{0,1:T(2,128)(2,1)S(1)}, bf16[2048,1]{0,1:T(2,128)(2,1)}, u32[]{:S(2)}) copy-start(bf16[2048,1]{0,1:T(2,128)(2,1)} %param.25) | copy-start | bytes 12292
  39.0 73.2 %reduce-scatter.5.cloned.1.call-start = ((), (), s32[]{:S(2)}) async-start(), calls=%async_computation.5 | async-start | bytes 655360 | tf_op jit(solution)/shard_map/reduce_scatter | solution.py:115
  112.2 12.8 %all-to-all-start.1 = ((bf16[8,16,512]{2,1,0:T(8,128)(2,1)}), bf16[8,16,512]{2,1,0:T(8,128)(2,1)S(1)}, u32[]{:S(2)}, u32[]{:S(2)}) async-start(bf16[8,16,512]{2,1,0:T(8,128)(2,1)} %reduce-scatter.5.cloned.1.call-done), calls=%async_computation.3 | async-start | bytes 262144 | tf_op jit(solution)/shard_map/all_to_all | solution.py:118
Sparse Core Ops, SparseCore 0:
  39.2 22.4 reduce-scatter.2
  93.0 19.1 reduce-scatter.4
